TPU v7x, 256 devices: a 4x2x16 block of a 4x16x16 slice. The times are simulated.
256 devices in a mesh: grp: 2 (over y), fs: 16 (over z), tp: 8 (over x, core).
Axes of the slice: x: 4, y: 2, z: 16, core: 2. Of those that a mesh axis runs over, the one named last changes fastest.
The devices are a block of a 4x16x16 slice.
Arguments:
- tokens: bfloat16 [32768, 2048], P(('grp', 'fs')), parts along dimension 0, may hold values from -1300 to 1300
- norm_gain: bfloat16 [2048], replicated, may hold values from 0.099609375 to 1.8984375
- gate_weight: bfloat16 [2048, 5120], P('fs', 'tp'), may hold values from -0.125 to 0.125
- up_weight: bfloat16 [2048, 5120], P('fs', 'tp'), may hold values from -0.125 to 0.125
- down_weight: bfloat16 [5120, 2048], P('tp', 'fs'), may hold values from -0.078125 to 0.078125
Outputs:
- mixed: bfloat16 [32768, 2048], P(('grp', 'fs', 'tp')), parts along dimension 0
There are 2 independent parts, one for each index of `grp`. A program takes and returns all parts, laid end to end along the dimension named above; an argument that names none is the same for every part. Nothing has to cross between parts.
All inputs are finite; a program needn't handle non-finite values.
Results may differ from a plain program's by a relative error of at most 0.013.
Values may be sent and summed in bfloat16 or wider, within the bound.
No kernel may reach another device: no remote copies, remote signals or barrier semaphores. Data moves between devices by JAX's collectives and lax.ppermute only.
A program may use at most 64 MiB of HBM per device.

v0:
```python
import jax
import jax.numpy as jnp
from jax import lax
from jax.sharding import PartitionSpec as P

EPSILON = 1e-06


def side_by_side(arrays, axis, dim, along):
    widths = [a.shape[along] for a in arrays]
    both = jnp.concatenate(arrays, axis=along)
    result = lax.all_gather(both, axis, axis=dim, tiled=True)
    return tuple(jnp.split(result, [sum(widths[:k]) for k in range(1, len(widths))], axis=along))


def normalize(tokens, norm_gain):
    as_float = tokens.astype(jnp.float32)
    scale = lax.rsqrt(jnp.mean(as_float * as_float, axis=-1, keepdims=True) + EPSILON)
    return (as_float * scale * norm_gain.astype(jnp.float32)).astype(jnp.bfloat16)


def rounded(values):
    return lax.optimization_barrier(values.astype(jnp.bfloat16)).astype(jnp.float32)


def on_device(tokens, norm_gain, gate_weight, up_weight, down_weight):
    normed = normalize(tokens, norm_gain)
    down_whole = lax.all_gather(down_weight, "fs", axis=1, tiled=True)
    gate_whole, up_whole = side_by_side((gate_weight, up_weight), "fs", 0, 1)
    gate_acts = jnp.dot(normed, gate_whole, preferred_element_type=jnp.float32)
    up_acts = jnp.dot(normed, up_whole, preferred_element_type=jnp.float32)
    hidden = (jax.nn.silu(gate_acts) * up_acts).astype(jnp.bfloat16)
    return lax.psum_scatter(
        rounded(jnp.dot(hidden, down_whole, preferred_element_type=jnp.float32)).astype(
            jnp.bfloat16
        ),
        "tp",
        scatter_dimension=0,
        tiled=True,
    )


def solution(mesh):
    return jax.shard_map(
        on_device,
        mesh=mesh,
        in_specs=(P(("grp", "fs"), None), P(), P("fs", "tp"), P("fs", "tp"), P("tp", "fs")),
        out_specs=P(("grp", "fs", "tp"), None),
        check_vma=False,
    )
```

profile of v0, /device:TPU:40, one launch (start us, length us, event | category | flops | bytes accessed | tf_op | source)
XLA Modules:
  0.0 240.0 jit_solution(12156880815646767167)
XLA Ops:
  6.5 0.0 all-gather.3.cloned.1.call-start
  6.6 1.7 pad_maximum_fusion
  8.3 0.1 all-gather.3.cloned.1.call-update
  8.4 0.1 all-gather.5.cloned.1.call-start
  8.4 0.7 all-gather.5.cloned.1.call-update
  9.2 0.1 reduce-scatter.2.cloned.1.call-start
  9.2 0.7 convert_element_type.18
  9.9 3.1 %fusion = f32[1024]{0:T(1024)S(1)} fusion(bf16[1024,2048]{1,0:T(8,128)(2,1)} %param.5), kind=kLoop, calls=%fused_computation.2 | loop fusion | flops 6290432 | bytes 4198400 | tf_op jit(solution)/shard_map/reduce_sum | solution.py:18
  13.0 88.4 %all-gather.3.cloned.1.call-done = bf16[2048,1280]{1,0:T(8,128)(2,1)} async-done(((bf16[128,1280]{1,0:T(8,128)(2,1)}), bf16[2048,1280]{1,0:T(8,128)(2,1)}) %all-gather.3.cloned.1.call-update) | async-done | bytes 5242896 | tf_op jit(solution)/shard_map/all_gather | solution.py:12
  101.4 6.3 %fusion.3 = f32[1024,640]{1,0:T(8,128)S(1)} fusion(bf16[2048,1280]{1,0:T(8,128)(2,1)} %all-gather.3.cloned.1.call-done, bf16[1024,2048]{1,0:T(8,128)(2,1)} %param.5, f32[2048]{0:T(1024)S(1)} %convert_element_type.18, f32[1024]{0:T(1024)S(1)} %add_rsqrt_fusion), kind=kOutput, calls=%fused_computation.6 | convolution fusion | flops 2692743168 | bytes 9449472 | tf_op jit(solution)/shard_map/dot_general | solution.py:31
  107.7 72.3 %all-gather.5.cloned.1.call-done = bf16[640,2048]{1,0:T(8,128)(2,1)} async-done(((bf16[640,128]{1,0:T(8,128)(2,1)}), bf16[640,2048]{1,0:T(8,128)(2,1)}) %all-gather.5.cloned.1.call-update) | async-done | bytes 2621456 | tf_op jit(solution)/shard_map/all_gather | solution.py:28
  180.0 12.9 %convolution_convert_fusion = bf16[1024,2048]{1,0:T(8,128)(2,1)} fusion(bf16[640,2048]{1,0:T(8,128)(2,1)} %all-gather.5.cloned.1.call-done, f32[1024,640]{1,0:T(8,128)S(1)} %fusion.3, bf16[2048,1280]{1,0:T(8,128)(2,1)} %all-gather.3.cloned.1.call-done, bf16[1024,2048]{1,0:T(8,128)(2,1)} %param.5, f32[2048]{0:T(1024)S(1)} %convert_element_type.18, ...), kind=kOutput, calls=%fused_computation.5 | convolution fusion | flops 5383127040 | bytes 16265216 | tf_op jit(solution)/shard_map/dot_general | solution.py:34
  192.9 0.1 reduce-scatter.2.cloned.1.call-update
  192.9 40.5 %reduce-scatter.2.cloned.1.call-done = bf16[128,2048]{1,0:T(8,128)(2,1)} async-done(((bf16[1024,2048]{1,0:T(8,128)(2,1)}), bf16[128,2048]{1,0:T(8,128)(2,1)}) %reduce-scatter.2.cloned.1.call-update) | async-done | bytes 524304 | tf_op jit(solution)/shard_map/reduce_scatter | solution.py:33
  (1 shorter events, 0.0 us)
Async XLA Ops:
  6.5 94.9 %all-gather.3.cloned.1.call-start = ((), (), s32[]{:S(2)}) async-start(), calls=%async_computation.1 | async-start | bytes 5570560 | tf_op jit(solution)/shard_map/all_gather | solution.py:12
  8.4 171.7 %all-gather.5.cloned.1.call-start = ((), (), s32[]{:S(2)}) async-start(), calls=%async_computation.2 | async-start | bytes 2785280 | tf_op jit(solution)/shard_map/all_gather | solution.py:28
  9.2 224.2 %reduce-scatter.2.cloned.1.call-start = ((), (), s32[]{:S(2)}) async-start(), calls=%async_computation.3 | async-start | bytes 4718592 | tf_op jit(solution)/shard_map/reduce_scatter | solution.py:33
Sparse Core Ops, SparseCore 0:
  9.1 92.2 all-gather.2
  103.2 76.7 all-gather.4
  193.0 40.3 reduce-scatter.1
where the time goes:
time: 240 us
  waiting for transfers between devices  202 us (84%)
  matrix products  19.1 us (8%)
  between operations  13.1 us (5%)
  other arithmetic  5.51 us (2%)
    all_gather x1, waiting for transfers between devices, side_by_side(): result = lax.all_gather(both, axis, axis=dim, tiled=True)  88.4 us
    all_gather x1, waiting for transfers between devices, on_device(): down_whole = lax.all_gather(down_weight, 'fs', axis=1, tiled=True)  72.3 us
    reduce_scatter x1, waiting for transfers between devices, on_device(): lax.psum_scatter(rounded(jnp.dot(hidden, down_whole, preferred_element_ty...  40.5 us
    dot_general x1, matrix products, on_device(): jnp.dot(hidden, down_whole, preferred_element_type=jnp.float32)  12.9 us
    dot_general x1, matrix products, on_device(): up_acts = jnp.dot(normed, up_whole, preferred_element_type=jnp.float32)  6.29 us
  transfers between devices with their start and end apart: 3, of which 3 were waited for; matrix products, arithmetic and copies ran while one was open for 4% of the time, Pallas kernels for 0%

commit v1 on v0

--- a/solution.py
+++ b/solution.py
@@ -1,9 +1,22 @@
+import functools
 import jax
 import jax.numpy as jnp
 from jax import lax
 from jax.sharding import PartitionSpec as P
 
 EPSILON = 1e-06
+
+
+def _report_screen(raw, link_axis, dim_k):
+    return jnp.concatenate(
+        lax.all_to_all(
+            jnp.stack(lax.axis_size(link_axis) * [raw], 0), link_axis, split_axis=0, concat_axis=0
+        ),
+        dim_k,
+    )
+
+
+_close_masks = functools.partial(_report_screen, link_axis="fs", dim_k=1)
 
 
 def side_by_side(arrays, axis, dim, along):
@@ -25,7 +38,7 @@
 
 def on_device(tokens, norm_gain, gate_weight, up_weight, down_weight):
     normed = normalize(tokens, norm_gain)
-    down_whole = lax.all_gather(down_weight, "fs", axis=1, tiled=True)
+    down_whole = _close_masks(down_weight)
     gate_whole, up_whole = side_by_side((gate_weight, up_weight), "fs", 0, 1)
     gate_acts = jnp.dot(normed, gate_whole, preferred_element_type=jnp.float32)
     up_acts = jnp.dot(normed, up_whole, preferred_element_type=jnp.float32)

time: 240 us -> 278 us (1.16)
  starting transfers between devices: 0.13 us -> 24 us
  waiting for transfers between devices: 202 us -> 212 us
  local copies, waits for them, and re-layouts: 0 us -> 2.89 us
    all_gather x1, waiting for transfers between devices: 88.4 us -> 170 us  [side_by_side(): result = lax.all_gather(both, axis, axis=dim, tiled=True)]
    all_gather x1 -> x0, waiting for transfers between devices: 72.3 us -> none  [on_device(): down_whole = lax.all_gather(down_weight, 'fs', axis=1, tiled=True)]
    all_to_all x0 -> x1, starting transfers between devices: none -> 24 us  [_report_screen(): lax.all_to_all(jnp.stack(lax.axis_size(link_axis) * [raw], 0), link_axis,...]
  transfers between devices with their start and end apart: 3 -> 3, of which waited for: 3 -> 2; matrix products, arithmetic and copies ran while one was open for 4% -> 5% of each run, Pallas kernels for 0% -> 0%
where the time goes in v1:
time: 278 us; the launch traced here: 277 us
  waiting for transfers between devices  212 us (76%)
  starting transfers between devices  24 us (9%)
  matrix products  20.3 us (7%)
  between operations  13.5 us (5%)
  other arithmetic  4.87 us (2%)
  local copies, waits for them, and re-layouts  2.89 us (1%)
    all_gather x1, waiting for transfers between devices, side_by_side(): result = lax.all_gather(both, axis, axis=dim, tiled=True)  170 us
    reduce_scatter x1, waiting for transfers between devices, on_device(): lax.psum_scatter(rounded(jnp.dot(hidden, down_whole, preferred_element_ty...  41.2 us
    all_to_all x1, starting transfers between devices, _report_screen(): lax.all_to_all(jnp.stack(lax.axis_size(link_axis) * [raw], 0), link_axis,...  24 us
    dot_general x1, matrix products, on_device(): jnp.dot(hidden, down_whole, preferred_element_type=jnp.float32)  12.4 us
    dot_general x1, matrix products, on_device(): up_acts = jnp.dot(normed, up_whole, preferred_element_type=jnp.float32)  7.95 us
  transfers between devices with their start and end apart: 3, of which 2 were waited for; matrix products, arithmetic and copies ran while one was open for 5% of the time, Pallas kernels for 0%

profile of v1, /device:TPU:40, one launch (start us, length us, event | category | flops | bytes accessed | tf_op | source)
XLA Modules:
  0.0 277.4 jit_solution(13340435810106685425)
XLA Ops:
  6.5 0.0 all-gather.2.cloned.1.call-start
  6.6 1.7 pad_maximum_fusion
  8.3 0.1 all-gather.2.cloned.1.call-update
  8.4 0.0 copy-start
  8.4 1.1 copy.6
  9.4 1.8 stack.2
  11.3 24.0 %all-to-all-start = ((bf16[16,640,128]{1,2,0:T(8,128)(2,1)}), bf16[16,640,128]{1,2,0:T(8,128)(2,1)S(1)}, u32[]{:S(2)}, u32[]{:S(2)}) async-start(bf16[16,640,128]{1,2,0:T(8,128)(2,1)} %stack.2), calls=%async_computation | async-start | bytes 5242880 | tf_op jit(solution)/shard_map/all_to_all | solution.py:12
  35.2 0.1 reduce-scatter.2.cloned.1.call-start
  35.3 0.0 copy-done
  35.3 3.1 %fusion = f32[1024]{0:T(1024)S(1)} fusion(bf16[1024,2048]{1,0:T(8,128)(2,1)} %param.5), kind=kLoop, calls=%fused_computation.2 | loop fusion | flops 6290432 | bytes 4198400 | tf_op jit(solution)/shard_map/reduce_sum | solution.py:31
  38.5 170.5 %all-gather.2.cloned.1.call-done = bf16[2048,1280]{1,0:T(8,128)(2,1)} async-done(((bf16[128,1280]{1,0:T(8,128)(2,1)}), bf16[2048,1280]{1,0:T(8,128)(2,1)}) %all-gather.2.cloned.1.call-update) | async-done | bytes 5242896 | tf_op jit(solution)/shard_map/all_gather | solution.py:25
  209.0 8.0 %fusion.3 = f32[1024,640]{1,0:T(8,128)} fusion(bf16[2048,1280]{1,0:T(8,128)(2,1)} %all-gather.2.cloned.1.call-done, bf16[1024,2048]{1,0:T(8,128)(2,1)} %param.5, f32[2048]{0:T(1024)S(1)} %convert_element_type.18, f32[1024]{0:T(1024)S(1)} %add_rsqrt_fusion), kind=kOutput, calls=%fused_computation.6 | convolution fusion | flops 2692743168 | bytes 9449472 | tf_op jit(solution)/shard_map/dot_general | solution.py:44
  216.9 0.0 all-to-all-done
  216.9 12.4 %convolution_convert_fusion = bf16[1024,2048]{1,0:T(8,128)(2,1)} fusion(bf16[640,2048]{0,1:T(8,128)(2,1)S(1)} %bitcast.4, f32[1024,640]{1,0:T(8,128)} %fusion.3, bf16[2048,1280]{1,0:T(8,128)(2,1)} %all-gather.2.cloned.1.call-done, bf16[1024,2048]{1,0:T(8,128)(2,1)} %param.5, f32[2048]{0:T(1024)S(1)} %convert_element_type.18, f32[1024]{0:T(1024)S(1)} %add_rsqrt_fusion), kind=kOutput, calls=%fused_computation.5 | convolution fusion | flops 5383127040 | bytes 16265216 | tf_op jit(solution)/shard_map/dot_general | solution.py:47
  229.3 0.1 reduce-scatter.2.cloned.1.call-update
  229.4 41.2 %reduce-scatter.2.cloned.1.call-done = bf16[128,2048]{1,0:T(8,128)(2,1)} async-done(((bf16[1024,2048]{1,0:T(8,128)(2,1)}), bf16[128,2048]{1,0:T(8,128)(2,1)}) %reduce-scatter.2.cloned.1.call-update) | async-done | bytes 524304 | tf_op jit(solution)/shard_map/reduce_scatter | solution.py:46
  (2 shorter events, 0.0 us)
Async XLA Ops:
  6.5 202.4 %all-gather.2.cloned.1.call-start = ((), (), s32[]{:S(2)}) async-start(), calls=%async_computation.2 | async-start | bytes 5570560 | tf_op jit(solution)/shard_map/all_gather | solution.py:25
  8.4 27.0 %copy-start = (bf16[2048]{0:T(1024)(128)(2,1)S(1)}, bf16[2048]{0:T(1024)(128)(2,1)}, u32[]{:S(2)}) copy-start(bf16[2048]{0:T(1024)(128)(2,1)} %param.6) | copy-start | bytes 12292
  11.3 205.7 %all-to-all-start = ((bf16[16,640,128]{1,2,0:T(8,128)(2,1)}), bf16[16,640,128]{1,2,0:T(8,128)(2,1)S(1)}, u32[]{:S(2)}, u32[]{:S(2)}) async-start(bf16[16,640,128]{1,2,0:T(8,128)(2,1)} %stack.2), calls=%async_computation | async-start | bytes 5242880 | tf_op jit(solution)/shard_map/all_to_all | solution.py:12
  35.2 235.3 %reduce-scatter.2.cloned.1.call-start = ((), (), s32[]{:S(2)}) async-start(), calls=%async_computation.3 | async-start | bytes 4718592 | tf_op jit(solution)/shard_map/reduce_scatter | solution.py:46
Sparse Core Ops, SparseCore 0:
  9.1 199.7 all-gather.1
  229.5 40.9 reduce-scatter.1
